TPU v7x, 256 devices: a 4x2x16 block of a 4x16x16 slice. The times are simulated.
256 devices in a mesh: grp: 2 (over y), sp: 32 (over z, core), tp: 4 (over x).
Axes of the slice: x: 4, y: 2, z: 16, core: 2. Of those that a mesh axis runs over, the one named last changes fastest.
The devices are a block of a 4x16x16 slice.
Arguments:
- queries_a: bfloat16 [16384, 2, 512], P(('grp', 'sp'), None, 'tp'), parts along dimension 0, may hold values from -120 to 120
- keys_a: bfloat16 [16384, 2, 512], P(('grp', 'sp'), None, 'tp'), parts along dimension 0, may hold values from -6 to 6
- values_a: bfloat16 [16384, 1024], P(('grp', 'sp'), 'tp'), parts along dimension 0, may hold values from -6 to 6
- queries_b: bfloat16 [16384, 2, 512], P(('grp', 'sp'), None, 'tp'), parts along dimension 0, may hold values from -120 to 120
- keys_b: bfloat16 [16384, 2, 512], P(('grp', 'sp'), None, 'tp'), parts along dimension 0, may hold values from -6 to 6
- values_b: bfloat16 [16384, 1024], P(('grp', 'sp'), 'tp'), parts along dimension 0, may hold values from -6 to 6
- lambdas: float32 [12], replicated, may hold values from 0.3 to 0.8
- head_gain_a: float32 [256], replicated, may hold values from 0.1 to 1.9
- head_gain_b: float32 [128], replicated, may hold values from 0.1 to 1.9
- out_a: bfloat16 [1024, 2048], P('tp'), may hold values from -0.125 to 0.125
- out_b: bfloat16 [1024, 2048], P('tp'), may hold values from -0.125 to 0.125
- residual: bfloat16 [16384, 2048], P(('grp', 'sp', 'tp')), parts along dimension 0, may hold values from -6 to 6
- gain_mix: float32 [2048], replicated, may hold values from 0.1 to 1.9
- gain_pre: float32 [2048], replicated, may hold values from 0.1 to 1.9
- gain_post: float32 [2048], replicated, may hold values from 0.1 to 1.9
- routes: int32 [16384, 4], P(('grp', 'sp', 'tp')), parts along dimension 0, may hold values from 0 to 31, all different within a row; in each aligned block of 64 rows (0 to 63, 64 to 127, ...) at most 10 rows name the same one
- route_weights: float32 [16384, 4], P(('grp', 'sp', 'tp')), parts along dimension 0, may hold values from 0.05 to 1
- expert_gate: bfloat16 [32, 2048, 2048], P('sp', None, 'tp'), may hold values from -1 to 1
- expert_up: bfloat16 [32, 2048, 2048], P('sp', None, 'tp'), may hold values from -1 to 1
- expert_down: bfloat16 [32, 2048, 2048], P('sp', 'tp'), may hold values from -0.125 to 0.125
Outputs:
- layer_out: bfloat16 [16384, 2048], P(('grp', 'sp', 'tp')), parts along dimension 0
There are 2 independent parts, one for each index of `grp`. A program takes and returns all parts, laid end to end along the dimension named above; an argument that names none is the same for every part. Nothing has to cross between parts.
Inputs may be any that keep to these rules, and one draw needn't show every extreme that they name: `routes`: in each aligned block of 64 rows (the rows of one device) no expert is named by more than 10 rows, a bound that some blocks reach.
All inputs are finite; a program needn't handle non-finite values.
Results may differ from a plain program's by a relative error of at most 0.018.
Values may be sent and summed in bfloat16 or wider, within the bound.
No kernel may reach another device: no remote copies, remote signals or barrier semaphores. Data moves between devices by JAX's collectives and lax.ppermute only.
A program may use at most 128 MiB of HBM per device.

v0:
```python
import jax
import jax.numpy as jnp
from jax import lax
from jax.sharding import PartitionSpec as P

HA = 4
DA = 128
DB = 64


def sent_together(arrays, axis, dim, along):
    columns = [a.reshape(*a.shape[:along], -1) for a in arrays]
    both = jnp.concatenate(columns, axis=along)
    filled, at, finished = (lax.all_gather(both, axis, axis=dim, tiled=True), 0, [])
    for a, column in zip(arrays, columns):
        slab = filled[..., at : at + column.shape[along]]
        finished.append(slab.reshape(*slab.shape[:along], *a.shape[along:]))
        at += column.shape[along]
    return tuple(finished)


def in_blocks(array, dim, devices):
    before, after = (array.shape[:dim], array.shape[dim + 1 :])
    return jnp.moveaxis(array.reshape(*before, devices, -1, *after), dim, 0)


def summed_on_arrival(array, axis, dim):
    devices = lax.axis_size(axis)
    blocks = lax.all_to_all(in_blocks(array, dim, devices), axis, 0, 0, tiled=True)
    return jnp.sum(blocks.astype(jnp.float32), axis=0)


def exchange_in_groups(array, axis, split_dim, concat_dim, work, item_dim, out_dim):
    items = jax.tree.leaves(array)[0].shape[item_dim]
    count = 2 if items % 2 == 0 else 1
    finished = []
    for k in range(count):
        group = jax.tree.map(
            lambda a: lax.slice_in_dim(
                a, k * (items // count), (k + 1) * (items // count), axis=item_dim
            ),
            array,
        )
        finished.append(
            work(
                lax.all_to_all(
                    group, axis, split_axis=split_dim, concat_axis=concat_dim, tiled=True
                )
            )
        )
    return jax.tree.map(lambda *parts: jnp.concatenate(parts, axis=out_dim), *finished)


def rms_norm(values, gain_vec):
    return values * lax.rsqrt(jnp.mean(values * values, -1, keepdims=True) + 1e-06) * gain_vec


def attend(current, query_rows, key_rows, value_rows, first_row, query_pos, head_size):
    run_max, run_sum, run_acc = current
    key_count = key_rows.shape[0]
    heads = query_rows.shape[2]
    key_view = key_rows.reshape(key_count, 2, heads, head_size)
    value_view = value_rows.reshape(key_count, heads, 2 * head_size)
    key_pos = first_row + jnp.arange(key_count, dtype=jnp.int32)
    visible = (key_pos[None, :] <= query_pos[:, None])[None, :, None, :]
    scores = jnp.einsum(
        "qmhd,kmhd->mqhk", query_rows, key_view, preferred_element_type=jnp.float32
    ) * head_size ** (-0.5)
    scores = jnp.where(visible, scores, -1e30)
    new_max = jnp.maximum(run_max, jnp.max(scores, -1))
    exp_terms = jnp.where(visible, jnp.exp(scores - new_max[..., None]), 0.0)
    rescale = jnp.exp(run_max - new_max)
    run_sum = run_sum * rescale + jnp.sum(exp_terms, -1)
    run_acc = run_acc * rescale[..., None] + jnp.einsum(
        "mqhk,khe->mqhe",
        exp_terms.astype(jnp.bfloat16),
        value_view,
        preferred_element_type=jnp.float32,
    )
    return (new_max, run_sum, run_acc)


def fresh_state(length, heads, head_size):
    return (
        jnp.full((2, length, heads), -1e30, jnp.float32),
        jnp.zeros((2, length, heads), jnp.float32),
        jnp.zeros((2, length, heads, 2 * head_size), jnp.float32),
    )


def finish(current, weights_two, gain_vec):
    run_max, run_sum, run_acc = current
    mixture = (
        run_acc[0] / run_sum[0][..., None]
        - weights_two[None, :, None] * run_acc[1] / run_sum[1][..., None]
    )
    normed = rms_norm(mixture, gain_vec)
    return normed.reshape(normed.shape[0], -1).astype(jnp.bfloat16)


def slot_numbers(flat_ids, experts):
    onehot = (flat_ids[:, None] == jnp.arange(experts, dtype=jnp.int32)[None, :]).astype(jnp.int32)
    before = jnp.cumsum(onehot, 0) - onehot
    return jnp.sum(before * onehot, 1)


def send_matrix(route_rows, experts, capacity):
    groups, sub_rows, top_count = route_rows.shape
    slot_ids = jax.vmap(lambda flat_ids: slot_numbers(flat_ids, experts))(
        route_rows.reshape(groups, -1)
    )
    group_ids = jnp.arange(groups, dtype=jnp.int32)[:, None]
    row_ids = (
        route_rows.reshape(groups, -1) * (groups * capacity) + group_ids * capacity + slot_ids
    ).reshape(-1)
    col_ids = jnp.broadcast_to(
        group_ids[:, :, None] * sub_rows + jnp.arange(sub_rows, dtype=jnp.int32)[None, :, None],
        route_rows.shape,
    ).reshape(-1)
    row_hot = (
        row_ids[:, None] == jnp.arange(experts * groups * capacity, dtype=jnp.int32)[None, :]
    ).astype(jnp.bfloat16)
    col_hot = (col_ids[:, None] == jnp.arange(groups * sub_rows, dtype=jnp.int32)[None, :]).astype(
        jnp.bfloat16
    )
    return jnp.einsum("ar,ac->rc", row_hot, col_hot, preferred_element_type=jnp.float32).astype(
        jnp.bfloat16
    )


def back_matrix(route_rows, route_weights, experts, capacity):
    sub_rows, top_count = route_rows.shape
    slot_ids = slot_numbers(route_rows.reshape(-1), experts)
    row_ids = route_rows.reshape(-1) * capacity + slot_ids
    col_ids = jnp.repeat(jnp.arange(sub_rows, dtype=jnp.int32), top_count)
    row_hot = (row_ids[:, None] == jnp.arange(experts * capacity, dtype=jnp.int32)[None, :]).astype(
        jnp.float32
    )
    tok_weighted = (col_ids[:, None] == jnp.arange(sub_rows, dtype=jnp.int32)[None, :]).astype(
        jnp.float32
    ) * route_weights.reshape(-1)[:, None]
    return jnp.einsum("at,ar->tr", tok_weighted, row_hot, precision=lax.Precision.HIGHEST)


def per_device(
    queries_a,
    keys_a,
    values_a,
    queries_b,
    keys_b,
    values_b,
    lambdas,
    head_gain_a,
    head_gain_b,
    out_a,
    out_b,
    residual,
    gain_mix,
    gain_pre,
    gain_post,
    routes,
    route_weights,
    expert_gate,
    expert_up,
    expert_down,
):
    length = queries_a.shape[0]
    heads_a = queries_a.shape[2] // DA
    heads_b = queries_b.shape[2] // DB
    head_slot = lax.axis_index("tp")
    seq_slot = lax.axis_index("sp")
    lambda_a = lax.dynamic_slice_in_dim(lambdas, head_slot * heads_a, heads_a)
    lambda_b = lax.dynamic_slice_in_dim(lambdas, HA + head_slot * heads_b, heads_b)
    groups = [
        (
            queries_a.reshape(length, 2, heads_a, DA),
            queries_b.reshape(length, 2, heads_b, DB),
            seq_slot * length + jnp.arange(length, dtype=jnp.int32),
            seq_slot * length + length - 1,
        )
    ]
    initial = tuple(
        (
            (
                fresh_state(group[2].shape[0], heads_a, DA),
                fresh_state(group[2].shape[0], heads_b, DB),
            )
            for group in groups
        )
    )
    pieces = sent_together((keys_a, values_a, keys_b, values_b), "sp", 0, 1)
    key_count = pieces[0].shape[0]
    span_rows = 1024

    def one_span(span_index, carried):
        offset = span_index * span_rows
        parts = tuple(
            (lax.dynamic_slice_in_dim(piece_part, offset, span_rows, 0) for piece_part in pieces)
        )
        group_qa, group_qb, group_pos, group_last = groups[0]

        def compute(inner, group_qa=group_qa, group_qb=group_qb, group_pos=group_pos):
            return (
                attend(inner[0], group_qa, parts[0], parts[1], offset, group_pos, DA),
                attend(inner[1], group_qb, parts[2], parts[3], offset, group_pos, DB),
            )

        updated = [lax.cond(offset <= group_last, compute, lambda inner: inner, carried[0])]
        return tuple(updated)

    final_state = lax.fori_loop(0, key_count // span_rows, one_span, initial)
    heads_out_a = finish(final_state[0][0], lambda_a, head_gain_a)
    heads_out_b = finish(final_state[0][1], lambda_b, head_gain_b)
    mixed_rows = summed_on_arrival(
        (
            jnp.dot(heads_out_a, out_a, preferred_element_type=jnp.float32)
            + jnp.dot(heads_out_b, out_b, preferred_element_type=jnp.float32)
        ).astype(jnp.bfloat16),
        "tp",
        0,
    )
    after_mix = (residual.astype(jnp.float32) + rms_norm(mixed_rows, gain_mix)).astype(jnp.bfloat16)
    normed = rms_norm(after_mix.astype(jnp.float32), gain_pre).astype(jnp.bfloat16)
    experts = lax.axis_size("sp")
    sub_rows = residual.shape[0]
    top_count = routes.shape[1]
    capacity = min(sub_rows, (5 * sub_rows * top_count + 4 * experts - 1) // (4 * experts))
    width = residual.shape[1]

    def expert_rows(piece_rows):
        gate_pre = jnp.dot(piece_rows, expert_gate[0], preferred_element_type=jnp.float32)
        up_pre = jnp.dot(piece_rows, expert_up[0], preferred_element_type=jnp.float32)
        glu_part = jnp.minimum(gate_pre, 7.0)
        lin_part = jnp.clip(up_pre, -7.0, 7.0)
        hidden = (glu_part * jax.nn.sigmoid(1.702 * glu_part) * (lin_part + 1.0)).astype(
            jnp.bfloat16
        )
        return jnp.dot(hidden, expert_down[0], preferred_element_type=jnp.float32)

    outgoing = jnp.dot(
        send_matrix(routes[None], experts, capacity), normed, preferred_element_type=jnp.float32
    ).astype(jnp.bfloat16)
    outgoing = outgoing.reshape(experts, capacity, width)

    def handle(arrived):
        sources, slot_count, columns = arrived.shape
        partials = expert_rows(
            lax.all_gather(arrived.reshape(-1, columns), "tp", axis=0, tiled=True)
        )
        mine = lax.psum_scatter(
            partials.astype(jnp.bfloat16), "tp", scatter_dimension=0, tiled=True
        )
        results = mine.reshape(sources, slot_count, columns)
        return lax.all_to_all(results, "sp", split_axis=0, concat_axis=0, tiled=True)

    returned = exchange_in_groups(outgoing, "sp", 0, 0, handle, 1, 1)
    combine = back_matrix(routes, route_weights, experts, capacity)
    routed = jnp.dot(
        combine,
        returned.reshape(-1, width).astype(jnp.float32),
        precision=lax.Precision.HIGHEST,
        preferred_element_type=jnp.float32,
    )
    return (after_mix.astype(jnp.float32) + rms_norm(routed, gain_post)).astype(jnp.bfloat16)


def solution(mesh):
    in_specs = (
        P(("grp", "sp"), None, "tp"),
        P(("grp", "sp"), None, "tp"),
        P(("grp", "sp"), "tp"),
        P(("grp", "sp"), None, "tp"),
        P(("grp", "sp"), None, "tp"),
        P(("grp", "sp"), "tp"),
        P(),
        P(),
        P(),
        P("tp", None),
        P("tp", None),
        P(("grp", "sp", "tp"), None),
        P(),
        P(),
        P(),
        P(("grp", "sp", "tp"), None),
        P(("grp", "sp", "tp"), None),
        P("sp", None, "tp"),
        P("sp", None, "tp"),
        P("sp", "tp", None),
    )
    out_specs = P(("grp", "sp", "tp"), None)
    return jax.shard_map(
        per_device, mesh=mesh, in_specs=in_specs, out_specs=out_specs, check_vma=False
    )
```

profile of v0, /device:TPU:33, one launch (start us, length us, event | category | flops | bytes accessed | tf_op | source)
XLA Modules:
  0.0 625.4 jit_solution(1137264615560985846)
XLA Ops:
  6.6 1.2 copy.33
  7.8 1.0 copy.34
  8.8 1.0 copy.35
  9.8 1.0 copy.36
  10.9 0.8 pad_maximum_fusion.1
  14.0 141.0 %all-gather.4.cloned.1.call-done = bf16[8192,1024]{0,1:T(8,128)(2,1)} async-done(((bf16[256,1024]{0,1:T(8,128)(2,1)}), bf16[8192,1024]{0,1:T(8,128)(2,1)}) %all-gather.4.cloned.1.call-update) | async-done | bytes 16777232 | tf_op jit(solution)/shard_map/all_gather | solution.py:14
  155.1 12.2 %fusion.140 = (bf16[8192,256]{0,1:T(8,128)(2,1)}, bf16[8192,256]{0,1:T(8,128)(2,1)}, bf16[8192,256]{0,1:T(8,128)(2,1)}, bf16[8192,256]{0,1:T(8,128)(2,1)}) fusion(bf16[8192,1024]{0,1:T(8,128)(2,1)} %all-gather.4.cloned.1.call-done), kind=kLoop, calls=%fused_computation.171 | loop fusion | bytes 33554432 | tf_op jit(solution)/shard_map/slice | solution.py:16
  167.3 6.4 %copy.39 = bf16[8192,2,128]{2,0,1:T(8,128)(2,1)} copy(bf16[8192,2,128]{0,2,1:T(8,128)(2,1)} %bitcast.235) | data formatting | bytes 8388608
  173.8 10.1 %while.24 = (s32[]{:T(128)}, f32[2,256,1]{1,0,2:T(2,128)S(1)}, f32[2,256,1]{1,0,2:T(2,128)S(1)}, f32[2,256,1,256]{1,3,0,2:T(8,128)S(1)}, f32[2,256,2]{1,2,0:T(2,...) while((s32[]{:T(128)}, f32[2,256,1]{1,0,2:T(2,128)S(1)}, ...), condition=%wide.region_7.8_spmd.clone, body=%wide.region_0.7_spmd.clone.sunk | while | flops 822350592 | bytes 27115984 | solution.py:211
  173.8 9.6 %conditional.3 = ((f32[2,256,1]{1,0,2:T(2,128)S(1)}, f32[2,256,1]{1,0,2:T(2,128)S(1)}, f32[2,256,1,256]{1,3,0,2:T(8,128)S(1)}, f32[2,256,2]{1,2,0:T(2,128)S(1)},...) conditional(s32[]{:T(128)} %convert_element_type.154, (f32[2,256,1]{1,0,2:T(2,128)S(1)}, ...), branch_computations={%region_1.0_spmd, %region_2.6_spmd} | conditional | flops 822350592 | bytes 27114610 | solution.py:208
  173.8 1.1 constant_dynamic-slice_fusion.1
  175.2 0.9 fusion.2
  176.1 1.1 fusion.3
  177.2 1.1 constant_dynamic-slice_fusion
  178.3 1.0 fusion.13
  179.3 1.5 fusion.7
  180.9 1.9 fusion.16
  184.6 1.2 copy.41
  186.1 0.9 fusion.108
  187.1 1.3 fusion.113
  188.6 1.5 fusion.35
  190.0 4.3 all-to-all-start
  195.5 13.4 %all-to-all-done = bf16[4,64,2048]{2,1,0:T(8,128)(2,1)S(1)} async-done(((bf16[4,64,2048]{2,1,0:T(8,128)(2,1)}), bf16[4,64,2048]{2,1,0:T(8,128)(2,1)S(1)}, u32[]{:S(2)}, u32[]{:S(2)}) %all-to-all-start) | async-done | bytes 1048608 | tf_op jit(solution)/shard_map/all_to_all | solution.py:29
  209.3 1.0 fusion.88
  210.3 1.8 convolution_convert_fusion.2
  212.0 1.6 reshape.498
  213.6 3.4 fusion.141
  217.0 126.5 %all_to_all.25 = bf16[32,5,2048]{2,1,0:T(8,128)(2,1)S(1)} all-to-all(bf16[32,5,2048]{2,1,0:T(8,128)(2,1)S(1)} %get-tuple-element.566), channel_id=1, replica_groups=mesh['grp'=2,'sp'=32,'tp'=4] {'sp'}, dimensions={0} | all-to-all | bytes 1310720 | tf_op jit(solution)/shard_map/all_to_all | solution.py:46
  343.5 1.2 reshape.499
  344.7 59.9 %all_to_all.26 = bf16[32,5,2048]{2,1,0:T(8,128)(2,1)S(1)} all-to-all(bf16[32,5,2048]{2,1,0:T(8,128)(2,1)} %get-tuple-element.567), channel_id=1, replica_groups=mesh['grp'=2,'sp'=32,'tp'=4] {'sp'}, dimensions={0} | all-to-all | bytes 1310720 | tf_op jit(solution)/shard_map/all_to_all | solution.py:46
  404.7 1.1 reshape.501
  406.0 3.9 fusion.46
  409.9 7.3 %convolution_convert_fusion.1 = bf16[640,2048]{1,0:T(8,128)(2,1)} fusion(bf16[1,512,2048]{2,1,0:T(8,128)(2,1)S(1)} %copy-done, bf16[640,2048]{1,0:T(8,128)(2,1)} %all-gather.6.cloned.1.call-done, bf16[1,2048,512]{2,1,0:T(8,128)(2,1)} %param.42, f32[640,512]{1,0:T(8,128)S(1)} %fusion.46), kind=kOutput, calls=%fused_computation.45 | convolution fusion | flops 2688614400 | bytes 10747904 | tf_op jit(solution)/shard_map/dot_general | solution.py:238
  417.4 19.5 %all-gather.8.cloned.1.call-done = bf16[640,2048]{1,0:T(8,128)(2,1)} async-done(((bf16[160,2048]{1,0:T(8,128)(2,1)}), bf16[640,2048]{1,0:T(8,128)(2,1)}) %all-gather.8.cloned.1.call-update) | async-done | bytes 2621456 | tf_op jit(solution)/shard_map/all_gather | solution.py:248
  436.8 3.9 fusion.49
  440.7 6.9 %convolution_convert_fusion = bf16[640,2048]{1,0:T(8,128)(2,1)} fusion(bf16[1,512,2048]{2,1,0:T(8,128)(2,1)S(1)} %copy-done, bf16[640,2048]{1,0:T(8,128)(2,1)} %all-gather.8.cloned.1.call-done, bf16[1,2048,512]{2,1,0:T(8,128)(2,1)} %param.42, f32[640,512]{1,0:T(8,128)S(1)} %fusion.49), kind=kOutput, calls=%fused_computation.44 | convolution fusion | flops 2688614400 | bytes 10747904 | tf_op jit(solution)/shard_map/dot_general | solution.py:238
  447.7 31.9 %reduce-scatter.3.cloned.1.call-done = bf16[160,2048]{1,0:T(8,128)(2,1)} async-done(((bf16[640,2048]{1,0:T(8,128)(2,1)}), bf16[160,2048]{1,0:T(8,128)(2,1)}) %reduce-scatter.3.cloned.1.call-update) | async-done | bytes 655376 | tf_op jit(solution)/shard_map/reduce_scatter | solution.py:250
  479.6 2.2 reshape.500
  481.8 13.2 %all-to-all-start.2 = ((bf16[32,5,2048]{2,1,0:T(8,128)(2,1)}), bf16[32,5,2048]{2,1,0:T(8,128)(2,1)S(1)}, u32[]{:S(2)}, u32[]{:S(2)}) async-start(bf16[32,5,2048]{2,1,0:T(8,128)(2,1)} %reshape.500), calls=%async_computation.3 | async-start | bytes 2097152 | tf_op jit(solution)/shard_map/all_to_all | solution.py:254
  495.0 26.9 %reduce-scatter.5.cloned.1.call-done = bf16[160,2048]{1,0:T(8,128)(2,1)} async-done(((bf16[640,2048]{1,0:T(8,128)(2,1)}), bf16[160,2048]{1,0:T(8,128)(2,1)}) %reduce-scatter.5.cloned.1.call-update) | async-done | bytes 655376 | tf_op jit(solution)/shard_map/reduce_scatter | solution.py:250
  521.9 2.3 reshape.502
  524.1 26.3 %all-to-all-done.2 = bf16[32,5,2048]{2,1,0:T(8,128)(2,1)S(1)} async-done(((bf16[32,5,2048]{2,1,0:T(8,128)(2,1)}), bf16[32,5,2048]{2,1,0:T(8,128)(2,1)S(1)}, u32[]{:S(2)}, u32[]{:S(2)}) %all-to-all-start.2) | async-done | bytes 655392 | tf_op jit(solution)/shard_map/all_to_all | solution.py:254
  550.4 5.1 all-to-all-start.4
  556.2 54.9 %all-to-all-done.4 = bf16[32,5,2048]{2,1,0:T(8,128)(2,1)} async-done(((bf16[32,5,2048]{2,1,0:T(8,128)(2,1)}), bf16[32,5,2048]{2,1,0:T(8,128)(2,1)}, u32[]{:S(2)}, u32[]{:S(2)}) %all-to-all-start.4) | async-done | bytes 655392 | tf_op jit(solution)/shard_map/all_to_all | solution.py:254
  611.1 3.3 pad_maximum_fusion
  614.4 2.5 reshape.503
  616.9 1.0 multiply_reduce_fusion
  618.0 0.9 fusion.91
  (117 shorter events, 7.2 us)
Async XLA Ops:
  6.5 403.4 %copy-start = (bf16[1,512,2048]{2,1,0:T(8,128)(2,1)S(1)}, bf16[1,512,2048]{2,1,0:T(8,128)(2,1)}, u32[]{:S(2)}) copy-start(bf16[1,512,2048]{2,1,0:T(8,128)(2,1)} %param.43) | copy-start | bytes 6291460
  6.6 5.2 copy-start.11
  6.6 5.5 copy-start.6
  6.6 5.6 copy-start.7
  6.6 5.7 copy-start.15
  6.6 7.4 %copy-start.14 = (f32[128]{0:T(128)S(1)}, f32[128]{0:T(128)}, u32[]{:S(2)}) copy-start(f32[128]{0:T(128)} %param.32) | copy-start | bytes 1540
  6.6 148.5 %all-gather.4.cloned.1.call-start = ((), (), s32[]{:S(2)}) async-start(), calls=%async_computation.7 | async-start | bytes 17301504 | tf_op jit(solution)/shard_map/all_gather | solution.py:14
  183.8 0.8 copy-start.2
  183.9 3.1 copy-start.13
  185.9 1.2 copy-start.3
  187.1 1.5 copy-start.4
  190.0 19.2 %copy-start.5 = (bf16[64,2048]{1,0:T(8,128)(2,1)S(1)}, bf16[64,2048]{1,0:T(8,128)(2,1)}, u32[]{:S(2)}) copy-start(bf16[64,2048]{1,0:T(8,128)(2,1)} %param.35) | copy-start | bytes 786436
  190.0 19.2 %copy-start.8 = (f32[2048]{0:T(1024)S(1)}, f32[2048]{0:T(1024)}, u32[]{:S(2)}) copy-start(f32[2048]{0:T(1024)} %param.36) | copy-start | bytes 24580
  190.0 18.9 %all-to-all-start = ((bf16[4,64,2048]{2,1,0:T(8,128)(2,1)}), bf16[4,64,2048]{2,1,0:T(8,128)(2,1)S(1)}, u32[]{:S(2)}, u32[]{:S(2)}) async-start(bf16[4,64,2048]{2,1,0:T(8,128)(2,1)} %bitcast.241), calls=%async_computation | async-start | bytes 2097152 | tf_op jit(solution)/shard_map/all_to_all | solution.py:29
  194.3 16.0 %copy-start.9 = (f32[2048]{0:T(1024)S(1)}, f32[2048]{0:T(1024)}, u32[]{:S(2)}) copy-start(f32[2048]{0:T(1024)} %param.37) | copy-start | bytes 24580
  194.3 211.7 %all-gather.6.cloned.1.call-start = ((), (), s32[]{:S(2)}) async-start(), calls=%async_computation.8 | async-start | bytes 3276800 | tf_op jit(solution)/shard_map/all_gather | solution.py:248
  344.7 92.1 %all-gather.8.cloned.1.call-start = ((), (), s32[]{:S(2)}) async-start(), calls=%async_computation.10 | async-start | bytes 3276800 | tf_op jit(solution)/shard_map/all_gather | solution.py:248
  405.9 73.7 %reduce-scatter.3.cloned.1.call-start = ((), (), s32[]{:S(2)}) async-start(), calls=%async_computation.9 | async-start | bytes 3276800 | tf_op jit(solution)/shard_map/reduce_scatter | solution.py:250
  417.3 104.6 %reduce-scatter.5.cloned.1.call-start = ((), (), s32[]{:S(2)}) async-start(), calls=%async_computation.11 | async-start | bytes 3276800 | tf_op jit(solution)/shard_map/reduce_scatter | solution.py:250
  481.8 68.6 %all-to-all-start.2 = ((bf16[32,5,2048]{2,1,0:T(8,128)(2,1)}), bf16[32,5,2048]{2,1,0:T(8,128)(2,1)S(1)}, u32[]{:S(2)}, u32[]{:S(2)}) async-start(bf16[32,5,2048]{2,1,0:T(8,128)(2,1)} %reshape.500), calls=%async_computation.3 | async-start | bytes 2097152 | tf_op jit(solution)/shard_map/all_to_all | solution.py:254
  495.0 60.6 %copy-start.12 = (f32[64,4]{0,1:T(4,128)S(1)}, f32[64,4]{0,1:T(4,128)}, u32[]{:S(2)}) copy-start(f32[64,4]{0,1:T(4,128)} %param.40) | copy-start | bytes 3076
  550.4 60.7 %all-to-all-start.4 = ((bf16[32,5,2048]{2,1,0:T(8,128)(2,1)}), bf16[32,5,2048]{2,1,0:T(8,128)(2,1)}, u32[]{:S(2)}, u32[]{:S(2)}) async-start(bf16[32,5,2048]{2,1,0:T(8,128)(2,1)} %reshape.502), calls=%async_computation.6 | async-start | bytes 2097152 | tf_op jit(solution)/shard_map/all_to_all | solution.py:254
  614.4 3.6 copy-start.10
  616.9 1.1 copy-start.1
Sparse Core Ops, SparseCore 0:
  11.9 143.1 all-gather.3
  344.8 30.8 all-gather.5
  406.0 30.7 all-gather.7
  439.2 40.2 reduce-scatter.2
  482.0 39.8 reduce-scatter.4
where the time goes:
time: 628 us; the launch traced here: 625 us
  waiting for transfers between devices  314 us (50%)
  blocking collectives  186 us (30%)
  local copies, waits for them, and re-layouts  43.7 us (7%)
  matrix products  33.3 us (5%)
  starting transfers between devices  22.8 us (4%)
  between operations  13.6 us (2%)
  other arithmetic  10.9 us (2%)
    all_to_all x2, blocking collectives, exchange_in_groups(): lax.all_to_all(group, axis, split_axis=split_dim, concat_axis=concat_dim,...  186 us
    all_gather x1, waiting for transfers between devices, sent_together(): lax.all_gather(both, axis, axis=dim, tiled=True)  141 us
    all_to_all x2, waiting for transfers between devices, handle(): lax.all_to_all(results, 'sp', split_axis=0, concat_axis=0, tiled=True)  81.2 us
    reduce_scatter x2, waiting for transfers between devices, handle(): lax.psum_scatter(partials.astype(jnp.bfloat16), 'tp', scatter_dimension=0...  58.8 us
    all_gather x2, waiting for transfers between devices, handle(): lax.all_gather(arrived.reshape(-1, columns), 'tp', axis=0, tiled=True)  19.5 us
    all_to_all x2, starting transfers between devices, handle(): lax.all_to_all(results, 'sp', split_axis=0, concat_axis=0, tiled=True)  18.3 us
    dot_general x2, matrix products, expert_rows(): return jnp.dot(hidden, expert_down[0], preferred_element_type=jnp.float32)  14.2 us
    all_to_all x1, waiting for transfers between devices, summed_on_arrival(): lax.all_to_all(in_blocks(array, dim, devices), axis, 0, 0, tiled=True)  13.4 us
  transfers between devices with their start and end apart: 8, of which 7 were waited for; matrix products, arithmetic and copies ran while one was open for 5% of the time, Pallas kernels for 0%

commit v1 on v0

v1 whole, which is shorter than its diff:
```python
import functools
import jax
import jax.numpy as jnp
from jax import lax
from jax.experimental import pallas as pl
from jax.experimental.pallas import tpu as pltpu
from jax.sharding import PartitionSpec as P

HA = 4
DA = 128
DB = 64
LOG2E = 1.4426950408889634
JOINED = 4


def in_blocks(array, dim, devices):
    before, after = (array.shape[:dim], array.shape[dim + 1 :])
    return jnp.moveaxis(array.reshape(*before, devices, -1, *after), dim, 0)


def summed_on_arrival(array, axis, dim):
    devices = lax.axis_size(axis)
    blocks = lax.all_to_all(in_blocks(array, dim, devices), axis, 0, 0, tiled=True)
    return jnp.sum(blocks.astype(jnp.float32), axis=0)


def rms_norm(values, gain_vec):
    return values * lax.rsqrt(jnp.mean(values * values, -1, keepdims=True) + 1e-06) * gain_vec

def attn_kernel(n_units, n_sub, tile_rows, scale, slot_ref, lam_ref, q_ref, kv_ref, gain_ref, out_ref, m_ref, l_ref, acc_ref):
    t = pl.program_id(0)
    rows = q_ref.shape[2]
    slot = slot_ref[0]
    last = (slot * rows) // tile_rows
    heads = n_units // 2
    width = acc_ref.shape[1]
    blocks = tile_rows // rows

    @pl.when(t == 0)
    def _():
        m_ref[...] = jnp.full(m_ref.shape, -1e30, jnp.float32)
        l_ref[...] = jnp.zeros(l_ref.shape, jnp.float32)
        acc_ref[...] = jnp.zeros(acc_ref.shape, jnp.float32)

    def tile(masked):
        if masked:
            key_pos = t * tile_rows + lax.broadcasted_iota(jnp.int32, (tile_rows, rows), 0)
            query_pos = slot * rows + lax.broadcasted_iota(jnp.int32, (tile_rows, rows), 1)
            visible = key_pos <= query_pos
        for u in range(n_units):
            map_at, head = u // heads, u % heads
            keys = kv_ref[:, map_at * 128 : (map_at + 1) * 128]
            scores = jnp.dot(keys, q_ref[u], preferred_element_type=jnp.float32) * scale
            if masked:
                scores = jnp.where(visible, scores, -1e30)
            old = m_ref[u : u + 1]
            new = jnp.maximum(old, jnp.max(scores, axis=0, keepdims=True))
            terms = jnp.exp2(scores - new)
            shrink = jnp.exp2(old - new)
            m_ref[u : u + 1] = new
            l_ref[u : u + 1] = l_ref[u : u + 1] * shrink + jnp.sum(terms, axis=0, keepdims=True)
            terms = terms.astype(jnp.bfloat16)
            at = 256 + 0 * head
            vals = jnp.concatenate(
                [kv_ref[b * rows + head * width : b * rows + (head + 1) * width, at : at + rows] for b in range(blocks)],
                axis=1,
            )
            acc_ref[u] = acc_ref[u] * shrink + jnp.dot(vals, terms, preferred_element_type=jnp.float32)

    @pl.when(t < last)
    def _():
        tile(False)

    @pl.when(t == last)
    def _():
        tile(True)
        for head in range(heads):
            one, two = head, heads + head
            mix = acc_ref[one] / l_ref[one : one + 1] - lam_ref[head] * acc_ref[two] / l_ref[two : two + 1]
            mean = jnp.mean(mix * mix, axis=0, keepdims=True)
            normed = mix * lax.rsqrt(mean + 1e-6) * gain_ref[...]
            out_ref[:, head * width : (head + 1) * width] = normed.T.astype(jnp.bfloat16)


def attention(slot, lam, queries, kv, gain, head_size, tile_rows=512):
    rows, _, channels = queries.shape
    heads = channels // head_size
    width = 2 * head_size
    qt = jnp.transpose(queries, (1, 2, 0))
    keep = (jnp.arange(channels)[None, :] // head_size == jnp.arange(heads)[:, None])[None, :, :, None]
    units = jnp.where(keep, qt[:, None], jnp.zeros((), jnp.bfloat16)).reshape(2 * heads, channels, rows)
    keys = kv.shape[0]
    n_units = 2 * heads
    grid_spec = pltpu.PrefetchScalarGridSpec(
        num_scalar_prefetch=1,
        grid=(keys // tile_rows,),
        in_specs=[
            pl.BlockSpec(memory_space=pltpu.SMEM),
            pl.BlockSpec((n_units, channels, rows), lambda t, s: (0, 0, 0)),
            pl.BlockSpec((tile_rows, kv.shape[1]), lambda t, s: (jnp.minimum(t, (s[0] * rows) // tile_rows), 0)),
            pl.BlockSpec((width, 1), lambda t, s: (0, 0)),
        ],
        out_specs=pl.BlockSpec((rows, heads * width), lambda t, s: (0, 0)),
        scratch_shapes=[
            pltpu.VMEM((n_units, rows), jnp.float32),
            pltpu.VMEM((n_units, rows), jnp.float32),
            pltpu.VMEM((n_units, width, rows), jnp.float32),
        ],
    )
    flops = 2 * rows * keys * n_units * (channels + width) // 2
    return pl.pallas_call(
        functools.partial(attn_kernel, n_units, heads, tile_rows, head_size ** (-0.5) * LOG2E),
        grid_spec=grid_spec,
        out_shape=jax.ShapeDtypeStruct((rows, heads * width), jnp.bfloat16),
        cost_estimate=pl.CostEstimate(flops=flops, bytes_accessed=2 * keys * kv.shape[1], transcendentals=n_units * rows * keys),
        name="attend",
    )(slot.reshape(1), lam, units, kv, gain.reshape(width, 1))


def pack(keys, values):
    rows = keys.shape[0]
    return jnp.concatenate([keys.reshape(rows, -1), values.T], axis=1)


def ffn_kernel(x_ref, gate_ref, up_ref, down_ref, out_ref):
    x = x_ref[...]
    gate_pre = jnp.dot(x, gate_ref[0], preferred_element_type=jnp.float32)
    up_pre = jnp.dot(x, up_ref[0], preferred_element_type=jnp.float32)
    glu_part = jnp.minimum(gate_pre, 7.0)
    lin_part = jnp.clip(up_pre, -7.0, 7.0)
    hidden = (glu_part * jax.nn.sigmoid(1.702 * glu_part) * (lin_part + 1.0)).astype(jnp.bfloat16)
    out_ref[...] = jnp.dot(hidden, down_ref[0], preferred_element_type=jnp.float32).astype(jnp.bfloat16)


def ffn(x, gate, up, down, tile_rows):
    rows, width = x.shape
    hidden = gate.shape[2]
    return pl.pallas_call(
        ffn_kernel,
        grid=(rows // tile_rows,),
        in_specs=[
            pl.BlockSpec((tile_rows, width), lambda i: (i, 0)),
            pl.BlockSpec(gate.shape, lambda i: (0, 0, 0)),
            pl.BlockSpec(up.shape, lambda i: (0, 0, 0)),
            pl.BlockSpec(down.shape, lambda i: (0, 0, 0)),
        ],
        out_specs=pl.BlockSpec((tile_rows, width), lambda i: (i, 0)),
        out_shape=jax.ShapeDtypeStruct((rows, width), jnp.bfloat16),
        cost_estimate=pl.CostEstimate(
            flops=6 * rows * width * hidden, bytes_accessed=4 * rows * width + 6 * width * hidden, transcendentals=rows * hidden
        ),
        name="expert",
    )(x, gate, up, down)


def grouped_kernel(left_ref, right_ref, out_ref):
    out_ref[0] = jnp.dot(left_ref[0], right_ref[0], preferred_element_type=jnp.float32).astype(jnp.bfloat16)


def grouped_dot(left, right):
    groups, rows, depth = left.shape
    width = right.shape[2]
    return pl.pallas_call(
        grouped_kernel,
        grid=(groups,),
        in_specs=[
            pl.BlockSpec((1, rows, depth), lambda i: (i, 0, 0)),
            pl.BlockSpec((1, depth, width), lambda i: (i, 0, 0)),
        ],
        out_specs=pl.BlockSpec((1, rows, width), lambda i: (i, 0, 0)),
        out_shape=jax.ShapeDtypeStruct((groups, rows, width), jnp.bfloat16),
        cost_estimate=pl.CostEstimate(
            flops=2 * groups * rows * depth * width,
            bytes_accessed=2 * groups * (rows * depth + depth * width + rows * width),
            transcendentals=0,
        ),
        name="pick",
    )(left, right)


def slot_tables(info, top_count, expert, capacity, joined):
    sources, rows, _ = info.shape
    match = info[..., :top_count] == expert.astype(jnp.float32)
    hit = jnp.any(match, -1)
    weight = jnp.sum(jnp.where(match, info[..., top_count:], 0.0), -1)
    order = jnp.arange(rows)
    earlier = (order[None, :] < order[:, None])[None]
    before = jnp.sum(jnp.where(earlier & hit[:, None, :], 1, 0), -1)
    place = (jnp.arange(sources) % joined)[:, None] * capacity + before
    place = jnp.where(hit, place, -1).reshape(sources // joined, joined * rows)
    weight = weight.reshape(sources // joined, joined * rows)
    slots = jnp.arange(joined * capacity)
    picks = place[:, None, :] == slots[None, :, None]
    slot_weight = jnp.sum(jnp.where(picks, weight[:, None, :], 0.0), -1)
    puts = place[:, :, None] == slots[None, None, :]
    return picks.astype(jnp.bfloat16), puts.astype(jnp.bfloat16), slot_weight


def per_device(
    queries_a,
    keys_a,
    values_a,
    queries_b,
    keys_b,
    values_b,
    lambdas,
    head_gain_a,
    head_gain_b,
    out_a,
    out_b,
    residual,
    gain_mix,
    gain_pre,
    gain_post,
    routes,
    route_weights,
    expert_gate,
    expert_up,
    expert_down,
):
    heads_a = queries_a.shape[2] // DA
    heads_b = queries_b.shape[2] // DB
    head_slot = lax.axis_index("tp")
    seq_slot = lax.axis_index("sp")
    experts = lax.axis_size("sp")
    parts = lax.axis_size("tp")
    lambda_a = lax.dynamic_slice_in_dim(lambdas, head_slot * heads_a, heads_a)
    lambda_b = lax.dynamic_slice_in_dim(lambdas, HA + head_slot * heads_b, heads_b)
    sub_rows, width = residual.shape
    top_count = routes.shape[1]
    capacity = min(sub_rows, (5 * sub_rows * top_count + 4 * experts - 1) // (4 * experts))

    filled_a = lax.all_gather(pack(keys_a, values_a), "sp", axis=0, tiled=True)
    filled_b = lax.all_gather(pack(keys_b, values_b), "sp", axis=0, tiled=True)
    own_info = jnp.concatenate([routes.astype(jnp.float32), route_weights], axis=1)
    info = lax.all_gather(own_info, "sp", axis=0)
    picks, puts, slot_weight = slot_tables(info, top_count, seq_slot, capacity, JOINED)

    heads_out_a = attention(seq_slot, lambda_a, queries_a, filled_a, head_gain_a, DA)
    heads_out_b = attention(seq_slot, lambda_b, queries_b, filled_b, head_gain_b, DB)
    partial = (
        jnp.dot(heads_out_a, out_a, preferred_element_type=jnp.float32)
        + jnp.dot(heads_out_b, out_b, preferred_element_type=jnp.float32)
    ).astype(jnp.bfloat16)
    mixed_rows = summed_on_arrival(partial, "tp", 0)
    after_mix = (residual.astype(jnp.float32) + rms_norm(mixed_rows, gain_mix)).astype(jnp.bfloat16)
    normed = rms_norm(after_mix.astype(jnp.float32), gain_pre).astype(jnp.bfloat16)

    tokens = lax.all_gather(normed, "sp", axis=0, tiled=True)
    picked = grouped_dot(picks, tokens.reshape(experts // JOINED, JOINED * sub_rows, width))
    gathered = lax.all_gather(picked.reshape(-1, width), "tp", axis=0, tiled=True)
    partials = ffn(gathered, expert_gate, expert_up, expert_down, experts * capacity)
    mine = lax.psum_scatter(partials, "tp", scatter_dimension=0, tiled=True)
    scaled = (mine.astype(jnp.float32) * slot_weight.reshape(-1, 1)).astype(jnp.bfloat16)
    spread = grouped_dot(puts, scaled.reshape(experts // JOINED, JOINED * capacity, width))
    routed = lax.psum_scatter(spread.reshape(-1, width), "sp", scatter_dimension=0, tiled=True)
    routed = routed.astype(jnp.float32)
    return (after_mix.astype(jnp.float32) + rms_norm(routed, gain_post)).astype(jnp.bfloat16)


def solution(mesh):
    in_specs = (
        P(("grp", "sp"), None, "tp"),
        P(("grp", "sp"), None, "tp"),
        P(("grp", "sp"), "tp"),
        P(("grp", "sp"), None, "tp"),
        P(("grp", "sp"), None, "tp"),
        P(("grp", "sp"), "tp"),
        P(),
        P(),
        P(),
        P("tp", None),
        P("tp", None),
        P(("grp", "sp", "tp"), None),
        P(),
        P(),
        P(),
        P(("grp", "sp", "tp"), None),
        P(("grp", "sp", "tp"), None),
        P("sp", None, "tp"),
        P("sp", None, "tp"),
        P("sp", "tp", None),
    )
    out_specs = P(("grp", "sp", "tp"), None)
    return jax.shard_map(
        per_device, mesh=mesh, in_specs=in_specs, out_specs=out_specs, check_vma=False
    )
```

time: 628 us -> 582 us (0.927)
  waiting for transfers between devices: 314 us -> 428 us
  blocking collectives: 186 us -> 74.7 us
  Pallas kernels: 0 us -> 38.3 us
  local copies, waits for them, and re-layouts: 43.7 us -> 7.64 us
  matrix products: 33.3 us -> 3.08 us
  starting transfers between devices: 22.8 us -> 0.39 us
    all_to_all x2 -> x1, blocking collectives: 186 us -> 18.4 us  [summed_on_arrival(): lax.all_to_all(in_blocks(array, dim, devices), axis, 0, 0, tiled=True)]
    reduce_scatter x2, waiting for transfers between devices: 58.8 us -> 177 us  [the longest x1 117 us: per_device(): lax.psum_scatter(spread.reshape(-1, width), 'sp', scatter_dimension=0, ti...]
    all_to_all x3 -> x0, waiting for transfers between devices: 94.6 us -> none  [the longest x2 81.2 us: handle(): lax.all_to_all(results, 'sp', split_axis=0, concat_axis=0, tiled=True)]
    all_gather x3 -> x4, waiting for transfers between devices: 161 us -> 250 us  [the longest x1 84.6 us: per_device(): filled_a = lax.all_gather(pack(keys_a, values_a), 'sp', axis=0, tiled=True)]
    all_gather x0 -> x1, blocking collectives: none -> 56.3 us  [per_device(): info = lax.all_gather(own_info, 'sp', axis=0)]
    pallas_call x0 -> x5, Pallas kernels: none -> 38.3 us  [the longest x2 16.1 us: grouped_dot(): pl.pallas_call(grouped_kernel, grid=(groups,), in_specs=[pl.BlockSpec((1,...]
    dot_general x11 -> x0, matrix products: 30.6 us -> none  [the longest x2 14.2 us: expert_rows(): return jnp.dot(hidden, expert_down[0], preferred_element_type=jnp.float32)]
    all_to_all x3 -> x0, starting transfers between devices: 22.5 us -> none  [the longest x2 18.3 us: handle(): lax.all_to_all(results, 'sp', split_axis=0, concat_axis=0, tiled=True)]
  transfers between devices with their start and end apart: 8 -> 6, of which waited for: 7 -> 6; matrix products, arithmetic and copies ran while one was open for 5% -> 2% of each run, Pallas kernels for 0% -> 1%
where the time goes in v1:
time: 582 us; the launch traced here: 579 us
  waiting for transfers between devices  428 us (74%)
  blocking collectives  74.7 us (13%)
  Pallas kernels  38.3 us (7%)
  between operations  13.7 us (2%)
  other arithmetic  12.9 us (2%)
  local copies, waits for them, and re-layouts  7.64 us (1%)
    reduce_scatter x1, waiting for transfers between devices, per_device(): lax.psum_scatter(spread.reshape(-1, width), 'sp', scatter_dimension=0, ti...  117 us
    all_gather x1, waiting for transfers between devices, per_device(): filled_a = lax.all_gather(pack(keys_a, values_a), 'sp', axis=0, tiled=True)  84.6 us
    all_gather x1, waiting for transfers between devices, per_device(): filled_b = lax.all_gather(pack(keys_b, values_b), 'sp', axis=0, tiled=True)  70 us
    reduce_scatter x1, waiting for transfers between devices, per_device(): mine = lax.psum_scatter(partials, 'tp', scatter_dimension=0, tiled=True)  60.7 us
    all_gather x1, waiting for transfers between devices, per_device(): lax.all_gather(picked.reshape(-1, width), 'tp', axis=0, tiled=True)  59.2 us
    all_gather x1, blocking collectives, per_device(): info = lax.all_gather(own_info, 'sp', axis=0)  56.3 us
    all_gather x1, waiting for transfers between devices, per_device(): tokens = lax.all_gather(normed, 'sp', axis=0, tiled=True)  36.3 us
    all_to_all x1, blocking collectives, summed_on_arrival(): lax.all_to_all(in_blocks(array, dim, devices), axis, 0, 0, tiled=True)  18.4 us
  transfers between devices with their start and end apart: 6, of which 6 were waited for; matrix products, arithmetic and copies ran while one was open for 2% of the time, Pallas kernels for 1%

profile of v1, /device:TPU:33, one launch (start us, length us, event | category | flops | bytes accessed | tf_op | source)
XLA Modules:
  0.0 578.6 jit_solution(11435799546710468756)
XLA Ops:
  6.6 1.1 copy.39
  7.8 0.9 copy.49
  8.7 0.7 pad_maximum_fusion
  9.5 0.9 copy.48
  10.5 1.0 copy.42
  11.5 0.7 pad_maximum_fusion.1
  12.3 0.1 copy.41
  12.5 0.7 copy.43.gain_ref
  13.3 0.6 dynamic_slice.7.lam_ref
  13.9 0.7 dynamic_slice.6.lam_ref
  14.6 0.1 copy.38
  14.7 0.8 copy.40.gain_ref
  15.5 0.8 bitcast_select_fusion.q_ref
  16.4 0.7 select_bitcast_fusion.q_ref
  17.1 84.6 %all-gather.7.cloned.1.call-done.kv_ref = bf16[8192,512]{1,0:T(8,128)(2,1)} async-done(((bf16[256,512]{1,0:T(8,128)(2,1)}), bf16[8192,512]{1,0:T(8,128)(2,1)}) %all-gather.7.cloned.1.call-update) | async-done | bytes 8388624 | tf_op jit(solution)/shard_map/all_gather | solution.py:233
  101.7 4.2 attend.2
  105.9 1.3 fusion.15
  107.2 70.0 %all-gather.9.cloned.1.call-done.kv_ref = bf16[8192,512]{1,0:T(8,128)(2,1)} async-done(((bf16[256,512]{1,0:T(8,128)(2,1)}), bf16[8192,512]{1,0:T(8,128)(2,1)}) %all-gather.9.cloned.1.call-update) | async-done | bytes 8388624 | tf_op jit(solution)/shard_map/all_gather | solution.py:234
  177.2 4.5 attend.3
  181.7 1.7 fusion
  183.5 18.4 %all_to_all.5 = bf16[4,64,2048]{2,1,0:T(8,128)(2,1)S(1)} all-to-all(bf16[4,64,2048]{2,1,0:T(8,128)(2,1)S(1)} %bitcast.33), channel_id=1, replica_groups=mesh['grp'=2,'sp'=32,'tp'=4] {'tp'}, dimensions={0} | all-to-all | bytes 2097152 | tf_op jit(solution)/shard_map/all_to_all | solution.py:23
  201.9 0.2 convert_reduce_fusion
  202.1 0.1 multiply_reduce_fusion
  202.2 0.3 fusion.4
  202.5 0.1 copy-done.5
  202.6 0.8 fusion.6
  203.6 56.3 %all-gather.1 = f32[32,64,8]{1,2,0:T(8,128)S(1)} all-gather(f32[1,64,8]{1,2,0:T(8,128)S(1)} %maximum_bitcast_fusion), channel_id=2, replica_groups=mesh['grp'=2,'sp'=32,'tp'=4] {'sp'}, dimensions={0}, use_global_device_ids=true | all-gather | bytes 67584 | tf_op jit(solution)/shard_map/all_gather | solution.py:236
  259.9 0.1 fusion.9
  260.0 0.1 reduce_or.12
  260.1 0.6 select_reduce_fusion
  260.7 0.1 reduce_sum.68
  260.8 0.1 add.97
  260.9 0.1 add.98
  261.0 0.7 fusion.8.left_ref
  261.7 36.3 %all-gather.11.cloned.1.call-done = bf16[2048,2048]{1,0:T(8,128)(2,1)} async-done(((bf16[64,2048]{1,0:T(8,128)(2,1)}), bf16[2048,2048]{1,0:T(8,128)(2,1)}) %all-gather.11.cloned.1.call-update) | async-done | bytes 8388624 | tf_op jit(solution)/shard_map/all_gather | solution.py:249
  298.0 7.9 %pick.2 = bf16[8,40,2048]{2,1,0:T(8,128)(2,1)} custom-call(bf16[8,40,256]{2,1,0:T(8,128)(2,1)} %fusion.8.left_ref, bf16[8,256,2048]{2,1,0:T(8,128)(2,1)} %bitcast.30), custom_call_target="tpu_custom_call" | custom-call | flops 335544320 | bytes 9863168 | tf_op jit(solution)/shard_map/pick/pallas_call | solution.py:163
  306.0 59.2 %all-gather.13.cloned.1.call-done.x_ref = bf16[1280,2048]{1,0:T(8,128)(2,1)} async-done(((bf16[320,2048]{1,0:T(8,128)(2,1)}), bf16[1280,2048]{1,0:T(8,128)(2,1)}) %all-gather.13.cloned.1.call-update) | async-done | bytes 5242896 | tf_op jit(solution)/shard_map/all_gather | solution.py:251
  365.2 13.6 %expert.1 = bf16[1280,2048]{1,0:T(8,128)(2,1)} custom-call(bf16[1280,2048]{1,0:T(8,128)(2,1)} %all-gather.13.cloned.1.call-done.x_ref, bf16[1,2048,512]{2,1,0:T(8,128)(2,1)} %gate_ref.1, bf16[1,2048,512]{2,1,0:T(8,128)(2,1)} %up_ref.1, bf16[1,512,2048]{2,1,0:T(8,128)(2,1)} %down_ref.1), custom_call_target="tpu_custom_call" | custom-call | flops 8053063680 | bytes 16777216 | tf_op jit(solution)/shard_map/expert/pallas_call | solution.py:138
  378.9 0.1 broadcast_in_dim.100
  379.0 0.1 select_reduce_fusion.1
  379.1 0.1 mul.94
  379.2 1.2 fusion.1.left_ref
  380.3 60.7 %reduce-scatter.3.cloned.1.call-done = bf16[320,2048]{1,0:T(8,128)(2,1)} async-done(((bf16[1280,2048]{1,0:T(8,128)(2,1)}), bf16[320,2048]{1,0:T(8,128)(2,1)}) %reduce-scatter.3.cloned.1.call-update) | async-done | bytes 1310736 | tf_op jit(solution)/shard_map/reduce_scatter | solution.py:253
  441.1 2.7 multiply_convert_fusion
  443.8 8.2 %pick.3 = bf16[8,256,2048]{2,1,0:T(8,128)(2,1)} custom-call(bf16[8,256,40]{2,1,0:T(8,128)(2,1)} %fusion.1.left_ref, bf16[8,40,2048]{2,1,0:T(8,128)(2,1)} %bitcast.32), custom_call_target="tpu_custom_call" | custom-call | flops 335544320 | bytes 9863168 | tf_op jit(solution)/shard_map/pick/pallas_call | solution.py:163
  452.0 116.7 %reduce-scatter.5.cloned.1.call-done = bf16[64,2048]{1,0:T(8,128)(2,1)} async-done(((bf16[2048,2048]{1,0:T(8,128)(2,1)}), bf16[64,2048]{1,0:T(8,128)(2,1)}) %reduce-scatter.5.cloned.1.call-update) | async-done | bytes 262160 | tf_op jit(solution)/shard_map/reduce_scatter | solution.py:256
  568.8 1.1 fusion.2
  569.9 1.8 fusion.7
  (49 shorter events, 0.9 us)
Async XLA Ops:
  6.5 99.3 %copy-start = (bf16[256,2048]{1,0:T(8,128)(2,1)S(1)}, bf16[256,2048]{1,0:T(8,128)(2,1)}, u32[]{:S(2)}) copy-start(bf16[256,2048]{1,0:T(8,128)(2,1)} %param.29) | copy-start | bytes 3145732
  6.6 5.8 %copy-start.2 = (bf16[256,2,128]{2,1,0:T(2,128)(2,1)S(1)}, bf16[256,2,128]{2,1,0:T(2,128)(2,1)}, u32[]{:S(2)}) copy-start(bf16[256,2,128]{2,1,0:T(2,128)(2,1)} %param.23) | copy-start | bytes 393220
  6.6 6.0 %copy-start.10 = (f32[128]{0:T(128)S(1)}, f32[128]{0:T(128)}, u32[]{:S(2)}) copy-start(f32[128]{0:T(128)} %param.28) | copy-start | bytes 1540
  6.6 6.7 %copy-start.11 = (f32[12]{0:T(128)S(1)}, f32[12]{0:T(128)}, u32[]{:S(2)}) copy-start(f32[12]{0:T(128)} %param.26) | copy-start | bytes 148
  6.6 8.0 %copy-start.3 = (bf16[256,2,128]{2,1,0:T(2,128)(2,1)S(1)}, bf16[256,2,128]{2,1,0:T(2,128)(2,1)}, u32[]{:S(2)}) copy-start(bf16[256,2,128]{2,1,0:T(2,128)(2,1)} %param.20) | copy-start | bytes 393220
  6.6 8.1 %copy-start.9 = (f32[256]{0:T(256)S(1)}, f32[256]{0:T(256)}, u32[]{:S(2)}) copy-start(f32[256]{0:T(256)} %param.27) | copy-start | bytes 3076
  6.6 95.1 %all-gather.7.cloned.1.call-start = ((), (), s32[]{:S(2)}) async-start(), calls=%async_computation.3 | async-start | bytes 8650752 | tf_op jit(solution)/shard_map/all_gather | solution.py:233
  9.5 167.8 %all-gather.9.cloned.1.call-start = ((), (), s32[]{:S(2)}) async-start(), calls=%async_computation.4 | async-start | bytes 8650752 | tf_op jit(solution)/shard_map/all_gather | solution.py:234
  12.3 285.7 %all-gather.11.cloned.1.call-start = ((), (), s32[]{:S(2)}) async-start(), calls=%async_computation.5 | async-start | bytes 8650752 | tf_op jit(solution)/shard_map/all_gather | solution.py:249
  183.5 18.7 %copy-start.1 = (bf16[64,2048]{1,0:T(8,128)(2,1)S(1)}, bf16[64,2048]{1,0:T(8,128)(2,1)}, u32[]{:S(2)}) copy-start(bf16[64,2048]{1,0:T(8,128)(2,1)} %param.31) | copy-start | bytes 786436
  183.5 18.7 %copy-start.4 = (f32[2048]{0:T(1024)S(1)}, f32[2048]{0:T(1024)}, u32[]{:S(2)}) copy-start(f32[2048]{0:T(1024)} %param.32) | copy-start | bytes 24580
  201.9 0.7 copy-start.5
  201.9 1.7 copy-start.7
  201.9 1.7 copy-start.8
  203.5 161.7 %all-gather.13.cloned.1.call-start = ((), (), s32[]{:S(2)}) async-start(), calls=%async_computation.6 | async-start | bytes 6553600 | tf_op jit(solution)/shard_map/all_gather | solution.py:251
  305.9 135.1 %reduce-scatter.3.cloned.1.call-start = ((), (), s32[]{:S(2)}) async-start(), calls=%async_computation.7 | async-start | bytes 6553600 | tf_op jit(solution)/shard_map/reduce_scatter | solution.py:253
  378.8 190.0 %reduce-scatter.5.cloned.1.call-start = ((), (), s32[]{:S(2)}) async-start(), calls=%async_computation.8 | async-start | bytes 8650752 | tf_op jit(solution)/shard_map/reduce_scatter | solution.py:256
  452.0 117.9 %copy-start.6 = (f32[2048]{0:T(1024)S(1)}, f32[2048]{0:T(1024)}, u32[]{:S(2)}) copy-start(f32[2048]{0:T(1024)} %param.34) | copy-start | bytes 24580
Sparse Core Ops, SparseCore 0:
  9.6 92.0 all-gather.6
  103.6 73.6 all-gather.8
  203.6 94.3 all-gather.10
  306.1 59.0 all-gather.12
  378.9 62.0 reduce-scatter.2
  452.2 116.5 reduce-scatter.4
